TPU v7x, 512 devices: a whole 4x4x16 slice. The times are simulated.
512 devices in a mesh: fs: 16 (over y, x), tp: 32 (over z, core).
Axes of the slice: x: 4, y: 4, z: 16, core: 2. Of those that a mesh axis runs over, the one named last changes fastest.
Arguments:
- x_later: bfloat16 [6144, 2048], P('fs'), may hold values from -6 to 6
- x_earlier: bfloat16 [6144, 2048], P('fs'), may hold values from -6 to 6
- cot_hidden: bfloat16 [6144, 4096], P('fs', 'tp'), may hold values from -6 to 6
- w_gate: bfloat16 [2048, 4096], P('fs', 'tp'), may hold values from -0.125 to 0.125
- w_up: bfloat16 [2048, 4096], P('fs', 'tp'), may hold values from -0.125 to 0.125
- grad_gate: float32 [2048, 4096], P('fs', 'tp'), may hold values from -192 to 192
- grad_up: float32 [2048, 4096], P('fs', 'tp'), may hold values from -192 to 192
Outputs:
- hidden_later: bfloat16 [6144, 4096], P('fs', 'tp')
- grad_input: bfloat16 [6144, 2048], P('fs')
- new_grad_gate: float32 [2048, 4096], P('fs', 'tp')
- new_grad_up: float32 [2048, 4096], P('fs', 'tp')
All inputs are finite; a program needn't handle non-finite values.
Results may differ from a plain program's by a relative error of at most 0.018.
Values may be sent and summed in bfloat16 or wider, within the bound.
A program may use at most 64 MiB of HBM per device.

v0:
```python
import jax
import jax.numpy as jnp
from jax import lax
from jax.sharding import PartitionSpec as P


def contract_last(left, right):
    return lax.dot_general(
        left, right, (((1,), (1,)), ((), ())), preferred_element_type=jnp.float32
    )


def contract_first(left, right):
    return lax.dot_general(
        left, right, (((0,), (0,)), ((), ())), preferred_element_type=jnp.float32
    )


def per_device(x_later, x_earlier, cot_hidden, w_gate, w_up, grad_gate, grad_up):
    hidden_width = w_gate.shape[1]
    whole_gate, whole_up = (
        lax.all_gather(w_gate, "fs", axis=0, tiled=True),
        lax.all_gather(w_up, "fs", axis=0, tiled=True),
    )
    gate_later = jnp.dot(x_later, whole_gate, preferred_element_type=jnp.float32)
    up_later = jnp.dot(x_later, whole_up, preferred_element_type=jnp.float32)
    gate_earlier = jnp.dot(x_earlier, whole_gate, preferred_element_type=jnp.float32)
    up_earlier = jnp.dot(x_earlier, whole_up, preferred_element_type=jnp.float32)
    hidden_later = (jax.nn.silu(gate_later) * up_later).astype(jnp.bfloat16)
    sigma = jax.nn.sigmoid(gate_earlier)
    cotangent = cot_hidden.astype(jnp.float32)
    delta_up = (cotangent * gate_earlier * sigma).astype(jnp.bfloat16)
    delta_gate = (cotangent * up_earlier * sigma * (1.0 + gate_earlier * (1.0 - sigma))).astype(
        jnp.bfloat16
    )
    grad_share = lax.psum_scatter(
        (contract_last(delta_gate, whole_gate) + contract_last(delta_up, whole_up)).astype(
            jnp.bfloat16
        ),
        "tp",
        scatter_dimension=0,
        tiled=True,
    )
    grad_input = lax.all_gather(grad_share, "tp", axis=0, tiled=True)
    deltas = jnp.concatenate([delta_gate, delta_up], 1)
    summed = lax.psum_scatter(
        contract_first(x_earlier, deltas).astype(jnp.bfloat16),
        "fs",
        scatter_dimension=0,
        tiled=True,
    ).astype(jnp.float32)
    new_grad_gate = grad_gate + summed[:, :hidden_width]
    new_grad_up = grad_up + summed[:, hidden_width:]
    return (hidden_later, grad_input, new_grad_gate, new_grad_up)


def solution(mesh):
    placed = (
        P("fs", None),
        P("fs", None),
        P("fs", "tp"),
        P("fs", "tp"),
        P("fs", "tp"),
        P("fs", "tp"),
        P("fs", "tp"),
    )
    return jax.shard_map(
        per_device,
        mesh=mesh,
        in_specs=placed,
        out_specs=(P("fs", "tp"), P("fs", None), P("fs", "tp"), P("fs", "tp")),
        check_vma=False,
    )
```

profile of v0, /device:TPU:1, one launch (start us, length us, event | category | flops | bytes accessed | tf_op | source)
XLA Modules:
  0.0 242.5 jit_solution(5092972627354294884)
XLA Ops:
  8.0 0.0 copy-start
  8.0 0.0 reduce-scatter.6.cloned.1.call-start
  8.1 20.1 %all_gather.10 = bf16[2048,128]{1,0:T(8,128)(2,1)S(1)} all-gather(bf16[128,128]{1,0:T(8,128)(2,1)} %param.11), channel_id=1, replica_groups=mesh['fs'=16,'tp'=32] {'fs'}, dimensions={0}, use_global_device_ids=true | all-gather | bytes 557056 | tf_op jit(solution)/shard_map/all_gather | solution.py:23
  28.1 17.9 %all_gather.9 = bf16[2048,128]{1,0:T(8,128)(2,1)S(1)} all-gather(bf16[128,128]{1,0:T(8,128)(2,1)} %param.10), channel_id=1, replica_groups=mesh['fs'=16,'tp'=32] {'fs'}, dimensions={0}, use_global_device_ids=true | all-gather | bytes 557056 | tf_op jit(solution)/shard_map/all_gather | solution.py:22
  46.1 0.0 copy-start.9
  46.1 1.7 fusion.7
  47.8 0.6 fusion.5
  48.4 0.7 fusion.1
  49.1 1.3 copy.37
  50.4 0.0 reduce-scatter.6.cloned.1.call-update
  50.4 0.0 all-gather.3.cloned.1.call-start
  50.5 0.6 fusion.13
  51.1 0.5 copy-done.4
  51.5 0.6 add_convert_fusion
  52.1 0.0 copy-start.7
  52.1 0.0 copy-start.8
  52.2 74.8 %fusion = bf16[16,2048]{1,0:T(8,128)(2,1)S(1)} fusion(bf16[384,2048]{1,0:T(8,128)(2,1)S(1)} %add_convert_fusion), kind=kCustom, calls=%all-reduce-scatter | all-reduce-scatter fusion | flops 1048577 | bytes 1640448
  127.0 3.4 %collective-permute-start.6 = (bf16[16,2048]{1,0:T(8,128)(2,1)S(1)}, bf16[16,2048]{1,0:T(8,128)(2,1)S(1)}, u32[]{:S(2)}, u32[]{:S(2)}) collective-permute-start(bf16[16,2048]{1,0:T(8,128)(2,1)S(1)} %fusion), channel_id=1, source_target_pairs={{0,7},{1,8},{2,9},{3,10},{4,11},{5,12},{6,13},{7,14},{8,15},{9,16}... | collective-permute-start | bytes 196616
  130.4 4.5 %collective-permute-start.5 = (bf16[16,2048]{1,0:T(8,128)(2,1)S(1)}, bf16[16,2048]{1,0:T(8,128)(2,1)S(1)}, u32[]{:S(2)}, u32[]{:S(2)}) collective-permute-start(bf16[16,2048]{1,0:T(8,128)(2,1)S(1)} %fusion), channel_id=1, source_target_pairs={{0,6},{1,7},{2,8},{3,9},{4,10},{5,11},{6,12},{7,13},{8,14},{9,15},... | collective-permute-start | bytes 196616
  134.9 6.2 %collective-permute-start.7 = (bf16[12,2048]{1,0:T(8,128)(2,1)S(1)}, bf16[12,2048]{1,0:T(8,128)(2,1)S(1)}, u32[]{:S(2)}, u32[]{:S(2)}) collective-permute-start(bf16[12,2048]{1,0:T(8,128)(2,1)S(1)} %slice.10), channel_id=1, source_target_pairs={{0,8},{1,9},{2,10},{3,11},{4,12},{5,13},{6,14},{7,15},{8,16},{9,17... | collective-permute-start | bytes 147464
  141.1 1.7 collective-permute-start.4
  142.8 6.4 %collective-permute-start.3 = (bf16[16,2048]{1,0:T(8,128)(2,1)S(1)}, bf16[16,2048]{1,0:T(8,128)(2,1)S(1)}, u32[]{:S(2)}, u32[]{:S(2)}) collective-permute-start(bf16[16,2048]{1,0:T(8,128)(2,1)S(1)} %fusion), channel_id=1, source_target_pairs={{0,4},{1,5},{2,6},{3,7},{4,8},{5,9},{6,10},{7,11},{8,12},{9,13},{1... | collective-permute-start | bytes 196616
  149.3 0.0 collective-permute-done.7
  149.3 1.6 collective-permute-start.2
  150.9 0.0 collective-permute-done.6
  150.9 2.8 %collective-permute-start.1 = (bf16[16,2048]{1,0:T(8,128)(2,1)S(1)}, bf16[16,2048]{1,0:T(8,128)(2,1)S(1)}, u32[]{:S(2)}, u32[]{:S(2)}) collective-permute-start(bf16[16,2048]{1,0:T(8,128)(2,1)S(1)} %fusion), channel_id=1, source_target_pairs={{0,2},{1,3},{2,4},{3,5},{4,6},{5,7},{6,8},{7,9},{8,10},{9,11},{10,... | collective-permute-start | bytes 196616
  153.7 0.0 collective-permute-done.5
  153.7 2.2 collective-permute-start
  155.9 1.3 dynamic-slice.4
  157.8 0.0 collective-permute-done.4
  157.8 0.0 collective-permute-done.3
  157.9 0.0 collective-permute-done.2
  157.9 0.0 collective-permute-done.1
  157.9 0.0 collective-permute-done
  157.9 1.5 concatenate.4
  159.4 0.7 dynamic-slice_bitcast_fusion
  160.0 0.0 all-gather.3.cloned.1.call-update
  160.1 0.1 copy.32
  160.2 0.0 copy-done.8
  160.2 0.1 copy.31
  160.3 0.0 copy-start.6
  160.3 2.1 fusion.12
  162.4 1.2 fusion.4
  163.6 0.9 copy.38
  164.6 0.7 copy.33
  165.4 0.7 copy.34
  166.1 65.4 %all-gather.3.cloned.1.call-done = bf16[32,12,2048]{2,1,0:T(8,128)(2,1)} async-done(((bf16[1,12,2048]{2,1,0:T(8,128)(2,1)}), bf16[32,12,2048]{2,1,0:T(8,128)(2,1)}) %all-gather.3.cloned.1.call-update) | async-done | bytes 1572880 | tf_op jit(solution)/shard_map/all_gather | solution.py:44
  231.4 3.6 %reshape.9 = bf16[384,2048]{1,0:T(8,128)(2,1)} reshape(bf16[32,12,2048]{2,1,0:T(8,128)(2,1)} %all-gather.3.cloned.1.call-done) | data formatting | bytes 3145728
  (17 shorter events, 0.1 us)
Async XLA Ops:
  8.0 38.1 %copy-start = (bf16[384,2048]{1,0:T(8,128)(2,1)S(1)}, bf16[384,2048]{1,0:T(8,128)(2,1)}, u32[]{:S(2)}) copy-start(bf16[384,2048]{1,0:T(8,128)(2,1)} %param.8) | copy-start | bytes 4718596
  8.0 155.6 %reduce-scatter.6.cloned.1.call-start = ((), (), s32[]{:S(2)}) async-start(), calls=%async_computation.2 | async-start | bytes 1114112
  28.1 19.6 %copy-start.3 = (bf16[2048,128]{1,0:T(8,128)(2,1)}, bf16[2048,128]{1,0:T(8,128)(2,1)S(1)}, u32[]{:S(2)}) copy-start(bf16[2048,128]{1,0:T(8,128)(2,1)S(1)} %all_gather.10) | copy-start | bytes 1572868
  46.1 4.4 %copy-start.1 = (bf16[2048,128]{1,0:T(8,128)(2,1)}, bf16[2048,128]{1,0:T(8,128)(2,1)S(1)}, u32[]{:S(2)}) copy-start(bf16[2048,128]{1,0:T(8,128)(2,1)S(1)} %all_gather.9) | copy-start | bytes 1572868
  46.1 1.7 copy-start.9
  50.4 181.0 %all-gather.3.cloned.1.call-start = ((), (), s32[]{:S(2)}) async-start(), calls=%async_computation.1 | async-start | bytes 2162688 | tf_op jit(solution)/shard_map/all_gather | solution.py:44
  50.5 1.0 copy-start.4
  52.1 107.9 %copy-start.7 = (f32[128,128]{1,0:T(8,128)S(1)}, f32[128,128]{1,0:T(8,128)}, u32[]{:S(2)}) copy-start(f32[128,128]{1,0:T(8,128)} %param.13) | copy-start | bytes 196612
  52.1 108.0 %copy-start.8 = (f32[128,128]{1,0:T(8,128)S(1)}, f32[128,128]{1,0:T(8,128)}, u32[]{:S(2)}) copy-start(f32[128,128]{1,0:T(8,128)} %param.12) | copy-start | bytes 196612
  127.0 33.3 %copy-start.2 = (bf16[2048,128]{1,0:T(8,128)(2,1)S(1)}, bf16[2048,128]{1,0:T(8,128)(2,1)}, u32[]{:S(2)}) copy-start(bf16[2048,128]{1,0:T(8,128)(2,1)} %copy-done.1) | copy-start | bytes 1572868
  127.0 24.0 %collective-permute-start.6 = (bf16[16,2048]{1,0:T(8,128)(2,1)S(1)}, bf16[16,2048]{1,0:T(8,128)(2,1)S(1)}, u32[]{:S(2)}, u32[]{:S(2)}) collective-permute-start(bf16[16,2048]{1,0:T(8,128)(2,1)S(1)} %fusion), channel_id=1, source_target_pairs={{0,7},{1,8},{2,9},{3,10},{4,11},{5,12},{6,13},{7,14},{8,15},{9,16}... | collective-permute-start | bytes 196616
  130.4 23.3 %collective-permute-start.5 = (bf16[16,2048]{1,0:T(8,128)(2,1)S(1)}, bf16[16,2048]{1,0:T(8,128)(2,1)S(1)}, u32[]{:S(2)}, u32[]{:S(2)}) collective-permute-start(bf16[16,2048]{1,0:T(8,128)(2,1)S(1)} %fusion), channel_id=1, source_target_pairs={{0,6},{1,7},{2,8},{3,9},{4,10},{5,11},{6,12},{7,13},{8,14},{9,15},... | collective-permute-start | bytes 196616
  134.9 14.4 %collective-permute-start.7 = (bf16[12,2048]{1,0:T(8,128)(2,1)S(1)}, bf16[12,2048]{1,0:T(8,128)(2,1)S(1)}, u32[]{:S(2)}, u32[]{:S(2)}) collective-permute-start(bf16[12,2048]{1,0:T(8,128)(2,1)S(1)} %slice.10), channel_id=1, source_target_pairs={{0,8},{1,9},{2,10},{3,11},{4,12},{5,13},{6,14},{7,15},{8,16},{9,17... | collective-permute-start | bytes 147464
  141.1 16.7 %collective-permute-start.4 = (bf16[16,2048]{1,0:T(8,128)(2,1)S(1)}, bf16[16,2048]{1,0:T(8,128)(2,1)S(1)}, u32[]{:S(2)}, u32[]{:S(2)}) collective-permute-start(bf16[16,2048]{1,0:T(8,128)(2,1)S(1)} %fusion), channel_id=1, source_target_pairs={{0,5},{1,6},{2,7},{3,8},{4,9},{5,10},{6,11},{7,12},{8,13},{9,14},{... | collective-permute-start | bytes 196616
  142.8 15.0 %collective-permute-start.3 = (bf16[16,2048]{1,0:T(8,128)(2,1)S(1)}, bf16[16,2048]{1,0:T(8,128)(2,1)S(1)}, u32[]{:S(2)}, u32[]{:S(2)}) collective-permute-start(bf16[16,2048]{1,0:T(8,128)(2,1)S(1)} %fusion), channel_id=1, source_target_pairs={{0,4},{1,5},{2,6},{3,7},{4,8},{5,9},{6,10},{7,11},{8,12},{9,13},{1... | collective-permute-start | bytes 196616
  149.3 8.6 %collective-permute-start.2 = (bf16[16,2048]{1,0:T(8,128)(2,1)S(1)}, bf16[16,2048]{1,0:T(8,128)(2,1)S(1)}, u32[]{:S(2)}, u32[]{:S(2)}) collective-permute-start(bf16[16,2048]{1,0:T(8,128)(2,1)S(1)} %fusion), channel_id=1, source_target_pairs={{0,3},{1,4},{2,5},{3,6},{4,7},{5,8},{6,9},{7,10},{8,11},{9,12},{10... | collective-permute-start | bytes 196616
  150.9 6.9 %collective-permute-start.1 = (bf16[16,2048]{1,0:T(8,128)(2,1)S(1)}, bf16[16,2048]{1,0:T(8,128)(2,1)S(1)}, u32[]{:S(2)}, u32[]{:S(2)}) collective-permute-start(bf16[16,2048]{1,0:T(8,128)(2,1)S(1)} %fusion), channel_id=1, source_target_pairs={{0,2},{1,3},{2,4},{3,5},{4,6},{5,7},{6,8},{7,9},{8,10},{9,11},{10,... | collective-permute-start | bytes 196616
  153.7 4.2 %collective-permute-start = (bf16[16,2048]{1,0:T(8,128)(2,1)S(1)}, bf16[16,2048]{1,0:T(8,128)(2,1)S(1)}, u32[]{:S(2)}, u32[]{:S(2)}) collective-permute-start(bf16[16,2048]{1,0:T(8,128)(2,1)S(1)} %fusion), channel_id=1, source_target_pairs={{0,1},{1,2},{2,3},{3,4},{4,5},{5,6},{6,7},{7,8},{8,9},{9,10},{10,1... | collective-permute-start | bytes 196616
  159.4 3.0 %copy-start.5 = (bf16[2048,128]{1,0:T(8,128)(2,1)S(1)}, bf16[2048,128]{1,0:T(8,128)(2,1)}, u32[]{:S(2)}) copy-start(bf16[2048,128]{1,0:T(8,128)(2,1)} %copy-done.3) | copy-start | bytes 1572868
  160.3 2.1 copy-start.6
Sparse Core Ops, SparseCore 0:
  50.6 100.0 reduce-scatter.5
Sparse Core Ops, SparseCore 1:
  160.1 71.2 all-gather.2
where the time goes:
time: 243 us; the launch traced here: 242 us
  blocking collectives  113 us (47%)
  waiting for transfers between devices  65.4 us (27%)
  starting transfers between devices  28.9 us (12%)
  between operations  16.5 us (7%)
  local copies, waits for them, and re-layouts  11.4 us (5%)
  matrix products  7.43 us (3%)
    unnamed x1, blocking collectives  74.8 us
    all_gather x1, waiting for transfers between devices, per_device(): grad_input = lax.all_gather(grad_share, 'tp', axis=0, tiled=True)  65.4 us
    unnamed x9, starting transfers between devices  28.9 us
    all_gather x1, blocking collectives, per_device(): lax.all_gather(w_up, 'fs', axis=0, tiled=True)  20.1 us
    all_gather x1, blocking collectives, per_device(): lax.all_gather(w_gate, 'fs', axis=0, tiled=True)  17.9 us
    unnamed x31, local copies, waits for them, and re-layouts  11.4 us
  transfers between devices with their start and end apart: 10, of which 1 were waited for; matrix products, arithmetic and copies ran while one was open for 35% of the time, Pallas kernels for 0%

commit v1 on v0

--- a/solution.py
+++ b/solution.py
@@ -41,7 +41,10 @@
         scatter_dimension=0,
         tiled=True,
     )
-    grad_input = lax.all_gather(grad_share, "tp", axis=0, tiled=True)
+    raw_out = lax.axis_size("tp")
+    current_value = jnp.stack(raw_out * [grad_share], 0)
+    spare = lax.all_to_all(current_value, "tp", 0, 0)
+    grad_input = jnp.concatenate(spare, 0)
     deltas = jnp.concatenate([delta_gate, delta_up], 1)
     summed = lax.psum_scatter(
         contract_first(x_earlier, deltas).astype(jnp.bfloat16),

time: 243 us -> 279 us (1.15)
  waiting for transfers between devices: 65.4 us -> 90.2 us
  starting transfers between devices: 28.9 us -> 42 us
    unnamed x11 -> x10, waiting for transfers between devices: 0.06 us -> 85.6 us
    all_gather x1 -> x0, waiting for transfers between devices: 65.4 us -> none  [per_device(): grad_input = lax.all_gather(grad_share, 'tp', axis=0, tiled=True)]
    all_to_all x0 -> x1, starting transfers between devices: none -> 12.2 us  [per_device(): spare = lax.all_to_all(current_value, 'tp', 0, 0)]
    unnamed x31 -> x28, local copies, waits for them, and re-layouts: 11.4 us -> 6.72 us
    all_to_all x0 -> x1, waiting for transfers between devices: none -> 4.59 us  [per_device(): spare = lax.all_to_all(current_value, 'tp', 0, 0)]
    reshape x0 -> x1, local copies, waits for them, and re-layouts: none -> 3.6 us  [per_device(): grad_input = jnp.concatenate(spare, 0)]
  transfers between devices with their start and end apart: 10 -> 10, of which waited for: 1 -> 2; matrix products, arithmetic and copies ran while one was open for 35% -> 3% of each run, Pallas kernels for 0% -> 0%
where the time goes in v1:
time: 279 us; the launch traced here: 278 us
  blocking collectives  112 us (40%)
  waiting for transfers between devices  90.2 us (32%)
  starting transfers between devices  42 us (15%)
  between operations  15 us (5%)
  local copies, waits for them, and re-layouts  11.9 us (4%)
  matrix products  7.44 us (3%)
    unnamed x10, waiting for transfers between devices  85.6 us
    unnamed x1, blocking collectives  73.7 us
    unnamed x9, starting transfers between devices  29.7 us
    all_gather x1, blocking collectives, per_device(): lax.all_gather(w_up, 'fs', axis=0, tiled=True)  20.1 us
    all_gather x1, blocking collectives, per_device(): lax.all_gather(w_gate, 'fs', axis=0, tiled=True)  17.9 us
    all_to_all x1, starting transfers between devices, per_device(): spare = lax.all_to_all(current_value, 'tp', 0, 0)  12.2 us
    unnamed x28, local copies, waits for them, and re-layouts  6.72 us
  transfers between devices with their start and end apart: 10, of which 2 were waited for; matrix products, arithmetic and copies ran while one was open for 3% of the time, Pallas kernels for 0%

profile of v1, /device:TPU:1, one launch (start us, length us, event | category | flops | bytes accessed | tf_op | source)
XLA Modules:
  0.0 278.3 jit_solution(3751109749429655214)
XLA Ops:
  7.2 0.0 copy-start
  7.2 20.1 %all_gather.7 = bf16[2048,128]{1,0:T(8,128)(2,1)S(1)} all-gather(bf16[128,128]{1,0:T(8,128)(2,1)} %param.11), channel_id=1, replica_groups=mesh['fs'=16,'tp'=32] {'fs'}, dimensions={0}, use_global_device_ids=true | all-gather | bytes 557056 | tf_op jit(solution)/shard_map/all_gather | solution.py:23
  27.3 17.9 %all_gather.6 = bf16[2048,128]{1,0:T(8,128)(2,1)S(1)} all-gather(bf16[128,128]{1,0:T(8,128)(2,1)} %param.10), channel_id=1, replica_groups=mesh['fs'=16,'tp'=32] {'fs'}, dimensions={0}, use_global_device_ids=true | all-gather | bytes 557056 | tf_op jit(solution)/shard_map/all_gather | solution.py:22
  45.2 0.0 copy-start.8
  45.2 1.7 fusion.7
  46.9 0.6 fusion.5
  47.5 0.0 copy-done.1
  47.5 0.6 fusion.13
  48.1 0.6 add_convert_fusion
  48.7 73.7 %fusion = bf16[16,2048]{1,0:T(8,128)(2,1)S(1)} fusion(bf16[384,2048]{1,0:T(8,128)(2,1)S(1)} %add_convert_fusion), kind=kCustom, calls=%all-reduce-scatter | all-reduce-scatter fusion | flops 1048577 | bytes 1640448
  122.4 3.6 %collective-permute-start.6 = (bf16[16,2048]{1,0:T(8,128)(2,1)S(1)}, bf16[16,2048]{1,0:T(8,128)(2,1)S(1)}, u32[]{:S(2)}, u32[]{:S(2)}) collective-permute-start(bf16[16,2048]{1,0:T(8,128)(2,1)S(1)} %fusion), channel_id=1, source_target_pairs={{0,7},{1,8},{2,9},{3,10},{4,11},{5,12},{6,13},{7,14},{8,15},{9,16}... | collective-permute-start | bytes 196616
  126.0 4.3 %collective-permute-start.5 = (bf16[16,2048]{1,0:T(8,128)(2,1)S(1)}, bf16[16,2048]{1,0:T(8,128)(2,1)S(1)}, u32[]{:S(2)}, u32[]{:S(2)}) collective-permute-start(bf16[16,2048]{1,0:T(8,128)(2,1)S(1)} %fusion), channel_id=1, source_target_pairs={{0,6},{1,7},{2,8},{3,9},{4,10},{5,11},{6,12},{7,13},{8,14},{9,15},... | collective-permute-start | bytes 196616
  130.3 6.6 %collective-permute-start.7 = (bf16[12,2048]{1,0:T(8,128)(2,1)S(1)}, bf16[12,2048]{1,0:T(8,128)(2,1)S(1)}, u32[]{:S(2)}, u32[]{:S(2)}) collective-permute-start(bf16[12,2048]{1,0:T(8,128)(2,1)S(1)} %slice.10), channel_id=1, source_target_pairs={{0,8},{1,9},{2,10},{3,11},{4,12},{5,13},{6,14},{7,15},{8,16},{9,17... | collective-permute-start | bytes 147464
  136.9 1.3 collective-permute-start.4
  138.2 7.4 %collective-permute-start.3 = (bf16[16,2048]{1,0:T(8,128)(2,1)S(1)}, bf16[16,2048]{1,0:T(8,128)(2,1)S(1)}, u32[]{:S(2)}, u32[]{:S(2)}) collective-permute-start(bf16[16,2048]{1,0:T(8,128)(2,1)S(1)} %fusion), channel_id=1, source_target_pairs={{0,4},{1,5},{2,6},{3,7},{4,8},{5,9},{6,10},{7,11},{8,12},{9,13},{1... | collective-permute-start | bytes 196616
  145.5 0.0 collective-permute-done.7
  145.5 1.6 collective-permute-start.2
  147.2 0.0 collective-permute-done.6
  147.2 2.8 collective-permute-start.1
  150.0 0.0 collective-permute-done.5
  150.0 2.2 collective-permute-start
  152.2 1.3 dynamic-slice.4
  154.1 0.0 collective-permute-done.4
  154.1 0.0 collective-permute-done.3
  154.1 0.0 collective-permute-done.2
  154.1 0.0 collective-permute-done.1
  154.1 0.0 collective-permute-done
  154.1 1.5 concatenate.4
  155.6 1.6 stack.2
  157.2 12.2 %all-to-all-start = ((bf16[32,12,2048]{2,1,0:T(8,128)(2,1)}), bf16[32,12,2048]{2,1,0:T(8,128)(2,1)}, u32[]{:S(2)}, u32[]{:S(2)}) async-start(bf16[32,12,2048]{2,1,0:T(8,128)(2,1)} %stack.2), calls=%async_computation | async-start | bytes 4194304 | tf_op jit(solution)/shard_map/all_to_all | solution.py:46
  169.5 0.0 reduce-scatter.6.cloned.1.call-start
  169.5 0.7 fusion.1
  170.2 0.0 copy-start.6
  170.3 0.0 copy-start.7
  170.3 0.0 copy-start.2
  170.3 1.3 copy.37
  171.6 0.0 reduce-scatter.6.cloned.1.call-update
  171.6 0.1 copy.32
  171.7 0.1 copy.31
  171.8 0.0 copy-start.5
  171.8 2.1 fusion.12
  174.0 1.2 fusion.4
  175.2 85.6 %reduce-scatter.6.cloned.1.call-done = bf16[128,256]{1,0:T(8,128)(2,1)} async-done(((bf16[2048,256]{1,0:T(8,128)(2,1)}), bf16[128,256]{1,0:T(8,128)(2,1)}) %reduce-scatter.6.cloned.1.call-update) | async-done | bytes 65552
  260.8 0.9 copy.38
  261.8 0.7 copy.33
  262.5 0.7 copy.34
  263.2 4.6 %all-to-all-done = bf16[32,12,2048]{2,1,0:T(8,128)(2,1)} async-done(((bf16[32,12,2048]{2,1,0:T(8,128)(2,1)}), bf16[32,12,2048]{2,1,0:T(8,128)(2,1)}, u32[]{:S(2)}, u32[]{:S(2)}) %all-to-all-start) | async-done | bytes 1572896 | tf_op jit(solution)/shard_map/all_to_all | solution.py:46
  267.8 3.6 %reshape.13 = bf16[384,2048]{1,0:T(8,128)(2,1)} reshape(bf16[32,12,2048]{2,1,0:T(8,128)(2,1)} %all-to-all-done) | data formatting | bytes 3145728 | tf_op jit(solution)/shard_map/reshape | solution.py:47
  (15 shorter events, 0.1 us)
Async XLA Ops:
  7.2 38.0 %copy-start = (bf16[384,2048]{1,0:T(8,128)(2,1)S(1)}, bf16[384,2048]{1,0:T(8,128)(2,1)}, u32[]{:S(2)}) copy-start(bf16[384,2048]{1,0:T(8,128)(2,1)} %param.8) | copy-start | bytes 4718596
  27.3 20.8 %copy-start.3 = (bf16[2048,128]{1,0:T(8,128)(2,1)}, bf16[2048,128]{1,0:T(8,128)(2,1)S(1)}, u32[]{:S(2)}) copy-start(bf16[2048,128]{1,0:T(8,128)(2,1)S(1)} %all_gather.7) | copy-start | bytes 1572868
  45.2 2.3 copy-start.1
  45.2 1.7 copy-start.8
  122.4 24.8 %collective-permute-start.6 = (bf16[16,2048]{1,0:T(8,128)(2,1)S(1)}, bf16[16,2048]{1,0:T(8,128)(2,1)S(1)}, u32[]{:S(2)}, u32[]{:S(2)}) collective-permute-start(bf16[16,2048]{1,0:T(8,128)(2,1)S(1)} %fusion), channel_id=1, source_target_pairs={{0,7},{1,8},{2,9},{3,10},{4,11},{5,12},{6,13},{7,14},{8,15},{9,16}... | collective-permute-start | bytes 196616
  126.0 24.0 %collective-permute-start.5 = (bf16[16,2048]{1,0:T(8,128)(2,1)S(1)}, bf16[16,2048]{1,0:T(8,128)(2,1)S(1)}, u32[]{:S(2)}, u32[]{:S(2)}) collective-permute-start(bf16[16,2048]{1,0:T(8,128)(2,1)S(1)} %fusion), channel_id=1, source_target_pairs={{0,6},{1,7},{2,8},{3,9},{4,10},{5,11},{6,12},{7,13},{8,14},{9,15},... | collective-permute-start | bytes 196616
  130.3 15.3 %collective-permute-start.7 = (bf16[12,2048]{1,0:T(8,128)(2,1)S(1)}, bf16[12,2048]{1,0:T(8,128)(2,1)S(1)}, u32[]{:S(2)}, u32[]{:S(2)}) collective-permute-start(bf16[12,2048]{1,0:T(8,128)(2,1)S(1)} %slice.10), channel_id=1, source_target_pairs={{0,8},{1,9},{2,10},{3,11},{4,12},{5,13},{6,14},{7,15},{8,16},{9,17... | collective-permute-start | bytes 147464
  136.9 17.2 %collective-permute-start.4 = (bf16[16,2048]{1,0:T(8,128)(2,1)S(1)}, bf16[16,2048]{1,0:T(8,128)(2,1)S(1)}, u32[]{:S(2)}, u32[]{:S(2)}) collective-permute-start(bf16[16,2048]{1,0:T(8,128)(2,1)S(1)} %fusion), channel_id=1, source_target_pairs={{0,5},{1,6},{2,7},{3,8},{4,9},{5,10},{6,11},{7,12},{8,13},{9,14},{... | collective-permute-start | bytes 196616
  138.2 15.9 %collective-permute-start.3 = (bf16[16,2048]{1,0:T(8,128)(2,1)S(1)}, bf16[16,2048]{1,0:T(8,128)(2,1)S(1)}, u32[]{:S(2)}, u32[]{:S(2)}) collective-permute-start(bf16[16,2048]{1,0:T(8,128)(2,1)S(1)} %fusion), channel_id=1, source_target_pairs={{0,4},{1,5},{2,6},{3,7},{4,8},{5,9},{6,10},{7,11},{8,12},{9,13},{1... | collective-permute-start | bytes 196616
  145.5 8.6 %collective-permute-start.2 = (bf16[16,2048]{1,0:T(8,128)(2,1)S(1)}, bf16[16,2048]{1,0:T(8,128)(2,1)S(1)}, u32[]{:S(2)}, u32[]{:S(2)}) collective-permute-start(bf16[16,2048]{1,0:T(8,128)(2,1)S(1)} %fusion), channel_id=1, source_target_pairs={{0,3},{1,4},{2,5},{3,6},{4,7},{5,8},{6,9},{7,10},{8,11},{9,12},{10... | collective-permute-start | bytes 196616
  147.2 6.9 %collective-permute-start.1 = (bf16[16,2048]{1,0:T(8,128)(2,1)S(1)}, bf16[16,2048]{1,0:T(8,128)(2,1)S(1)}, u32[]{:S(2)}, u32[]{:S(2)}) collective-permute-start(bf16[16,2048]{1,0:T(8,128)(2,1)S(1)} %fusion), channel_id=1, source_target_pairs={{0,2},{1,3},{2,4},{3,5},{4,6},{5,7},{6,8},{7,9},{8,10},{9,11},{10,... | collective-permute-start | bytes 196616
  150.0 4.2 %collective-permute-start = (bf16[16,2048]{1,0:T(8,128)(2,1)S(1)}, bf16[16,2048]{1,0:T(8,128)(2,1)S(1)}, u32[]{:S(2)}, u32[]{:S(2)}) collective-permute-start(bf16[16,2048]{1,0:T(8,128)(2,1)S(1)} %fusion), channel_id=1, source_target_pairs={{0,1},{1,2},{2,3},{3,4},{4,5},{5,6},{6,7},{7,8},{8,9},{9,10},{10,1... | collective-permute-start | bytes 196616
  157.2 110.6 %all-to-all-start = ((bf16[32,12,2048]{2,1,0:T(8,128)(2,1)}), bf16[32,12,2048]{2,1,0:T(8,128)(2,1)}, u32[]{:S(2)}, u32[]{:S(2)}) async-start(bf16[32,12,2048]{2,1,0:T(8,128)(2,1)} %stack.2), calls=%async_computation | async-start | bytes 4194304 | tf_op jit(solution)/shard_map/all_to_all | solution.py:46
  169.5 91.3 %reduce-scatter.6.cloned.1.call-start = ((), (), s32[]{:S(2)}) async-start(), calls=%async_computation.2 | async-start | bytes 1114112
  170.2 1.4 copy-start.6
  170.3 1.5 copy-start.7
  170.3 1.6 copy-start.2
  171.6 2.4 copy-start.4
  171.8 2.1 copy-start.5
Sparse Core Ops, SparseCore 0:
  174.9 85.7 reduce-scatter.5
